TPU v7x, 128 devices: a whole 4x4x4 slice. The times are simulated.
128 devices in a mesh: fs: 16 (over z, y), tp: 4 (over x), rep: 2 (over core).
Axes of the slice: x: 4, y: 4, z: 4, core: 2. Of those that a mesh axis runs over, the one named last changes fastest.
Arguments:
- gate_grads: float32 [2, 5632, 2048], P('rep', 'fs', 'tp'), may hold values from -16 to 16, as said below
- gate_velocity: float32 [5632, 2048], P(('fs', 'rep'), 'tp'), may hold values from -31 to 31, as said below
- gate_weight: float32 [5632, 2048], P(('fs', 'rep'), 'tp'), may hold values from -4 to 4
- up_grads: float32 [2, 5632, 2048], P('rep', 'fs', 'tp'), may hold values from -16 to 16, as said below
- up_velocity: float32 [5632, 2048], P(('fs', 'rep'), 'tp'), may hold values from -31 to 31, as said below
- up_weight: float32 [5632, 2048], P(('fs', 'rep'), 'tp'), may hold values from -4 to 4
- branch_grads: float32 [2, 2048, 1024], P('rep', 'fs', 'tp'), may hold values from -16 to 16, as said below
- branch_velocity: float32 [2048, 1024], P(('fs', 'rep'), 'tp'), may hold values from -31 to 31, as said below
- branch_weight: float32 [2048, 1024], P(('fs', 'rep'), 'tp'), may hold values from -4 to 4
Outputs:
- gate_momentum: float32 [5632, 2048], P(('fs', 'rep'), 'tp')
- gate_updated: float32 [5632, 2048], P(('fs', 'rep'), 'tp')
- up_momentum: float32 [5632, 2048], P(('fs', 'rep'), 'tp')
- up_updated: float32 [5632, 2048], P(('fs', 'rep'), 'tp')
- branch_momentum: float32 [2048, 1024], P(('fs', 'rep'), 'tp')
- branch_updated: float32 [2048, 1024], P(('fs', 'rep'), 'tp')
Inputs may be any that keep to these rules, and one draw needn't show every extreme that they name: `gate_grads`: entries vary in scale over rows and over columns. `up_grads`: entries vary in scale over rows and over columns. `branch_grads`: entries vary in scale over rows and over columns. `gate_velocity`: entries vary in scale over rows and over columns. `up_velocity`: entries vary in scale over rows and over columns. `branch_velocity`: entries vary in scale over rows and over columns.
All inputs are finite; a program needn't handle non-finite values.
Results may differ from a plain program's by a relative error of at most 0.039.
Values may be sent and summed in bfloat16 or wider, within the bound.
A program may use at most 64 MiB of HBM per device.

v0:
```python
import math
import jax
import jax.numpy as jnp
from jax import lax
from jax.sharding import Mesh
from jax.sharding import PartitionSpec as P

D = 2048
FF = 5632
ITERS = 3
FS_REP = ("fs_0", "fs_1", "rep")
FS_TP_REP = ("fs_0", "fs_1", "tp", "rep")
FS = ("fs_0", "fs_1")
MOMENT = 0.95
COEF_ONE = 3.4445
COEF_THREE = -4.775
COEF_FIVE = 2.0315
SAFETY = 2.0
RATE = 0.5
SHRINK = 0.95


def joined_along(tiles, dim):
    lengths = list(tiles.shape[1:])
    lengths[dim] *= tiles.shape[0]
    return jnp.moveaxis(tiles, 0, dim).reshape(lengths)


def from_everyone(value, axis):
    devices = lax.axis_size(axis)
    return lax.all_to_all(
        jnp.broadcast_to(value[None], (devices, *value.shape)), axis, 0, 0, tiled=True
    )


def gathered_copies(value, axis, dim):
    return joined_along(from_everyone(value, axis), dim)


def split_up(value, dim, devices):
    before, after = (value.shape[:dim], value.shape[dim + 1 :])
    return jnp.moveaxis(value.reshape(*before, devices, -1, *after), dim, 0)


def sum_at_owner(value, axis, dim):
    devices = lax.axis_size(axis)
    tiles = lax.all_to_all(split_up(value, dim, devices), axis, 0, 0, tiled=True)
    return jnp.sum(tiles.astype(jnp.float32), axis=0)


def by_axis(value, axes):
    for axis in axes:
        value = lax.psum(value, axis)
    return value


def side_by_side(arrays, axis, dim, along):
    ends, at = ([], 0)
    for a in arrays[:-1]:
        at += a.shape[along]
        ends.append(at)
    both = jnp.concatenate(arrays, axis=along)
    return tuple(jnp.split(sum_at_owner(both, axis, dim), ends, axis=along))


def rounded(part):
    narrow = lax.optimization_barrier(part.astype(jnp.bfloat16))
    return narrow.astype(jnp.float32)


def gram(current):
    whole = gathered_copies(current, "tp", 1)
    part = lax.dot_general(
        whole, current, (((0,), (0,)), ((), ())), preferred_element_type=jnp.float32
    )
    share = sum_at_owner(rounded(part).astype(jnp.bfloat16), FS_REP, 0)
    return (whole, share)


def spread(share):
    return lax.all_gather(share, FS_REP, axis=0, tiled=True)


def second_product(ymat, columns):
    return jnp.dot(gathered_copies(ymat, "tp", 1), columns, preferred_element_type=jnp.float32)


def combine(current, ymat, zmat, factor):
    mixed = COEF_ONE * factor * current.astype(jnp.float32) + COEF_THREE * ymat.astype(jnp.float32)
    return (mixed + COEF_FIVE * zmat.astype(jnp.float32)).astype(jnp.bfloat16)


def orthogonalize(starts):
    firsts = [gram(current) for current in starts]
    squares = tuple((jnp.sum(jnp.square(current.astype(jnp.float32))) for current in starts))
    seconds = tuple((jnp.sum(share * share) for whole, share in firsts))
    totals = jax.tree.map(lambda part: by_axis(part, FS_TP_REP), squares + seconds)
    first_sums, gram_sums = (totals[:3], totals[3:])
    finals = []
    for current, pair, first_sum, gram_sum in zip(starts, firsts, first_sums, gram_sums):
        whole, share = pair
        ratio = SAFETY * (gram_sum + 1.0) / (first_sum + 1.0)
        factor = lax.rsqrt(ratio)
        columns = spread((share / ratio).astype(jnp.bfloat16))
        ymat = (jnp.dot(whole, columns, preferred_element_type=jnp.float32) * factor).astype(
            jnp.bfloat16
        )
        zmat = second_product(ymat, columns).astype(jnp.bfloat16)
        current = combine(current, ymat, zmat, factor)
        for index in range(ITERS - 1):
            whole, share = gram(current)
            columns = spread(share.astype(jnp.bfloat16))
            ymat = jnp.dot(whole, columns, preferred_element_type=jnp.float32).astype(jnp.bfloat16)
            zmat = second_product(ymat, columns).astype(jnp.bfloat16)
            current = combine(current, ymat, zmat, 1.0)
        finals.append(current)
    return tuple(finals)


def local(
    gate_grads,
    gate_velocity,
    gate_weight,
    up_grads,
    up_velocity,
    up_weight,
    branch_grads,
    branch_velocity,
    branch_weight,
):
    totals = (
        *side_by_side(
            (gate_grads.astype(jnp.bfloat16), up_grads.astype(jnp.bfloat16)), "rep", 1, 0
        ),
        sum_at_owner(branch_grads.astype(jnp.bfloat16), "rep", 1),
    )
    velocities = (gate_velocity, up_velocity, branch_velocity)
    moments = [MOMENT * velocity + total[0] for velocity, total in zip(velocities, totals)]
    starts = tuple((moment.astype(jnp.bfloat16) for moment in moments))
    finals = orthogonalize(starts)
    weights = (gate_weight, up_weight, branch_weight)
    heights = (FF, FF, D)
    results = []
    for moment, weight, final, height in zip(moments, weights, finals, heights):
        results.append(moment)
        results.append(SHRINK * weight - RATE * math.sqrt(height) * final.astype(jnp.float32))
    return tuple(results)


def solution(mesh):
    torus = Mesh(
        mesh.devices.reshape(4, 4, mesh.shape["tp"], mesh.shape["rep"]),
        ("fs_0", "fs_1", "tp", "rep"),
    )
    return jax.shard_map(
        local,
        mesh=torus,
        in_specs=(
            P("rep", FS, "tp"),
            P(FS_REP, "tp"),
            P(FS_REP, "tp"),
            P("rep", FS, "tp"),
            P(FS_REP, "tp"),
            P(FS_REP, "tp"),
            P("rep", FS, "tp"),
            P(FS_REP, "tp"),
            P(FS_REP, "tp"),
        ),
        out_specs=(
            P(FS_REP, "tp"),
            P(FS_REP, "tp"),
            P(FS_REP, "tp"),
            P(FS_REP, "tp"),
            P(FS_REP, "tp"),
            P(FS_REP, "tp"),
        ),
        check_vma=False,
    )
```

profile of v0, /device:TPU:0, one launch (start us, length us, event | category | flops | bytes accessed | tf_op | source)
XLA Modules:
  0.0 692.4 jit_solution(9970207772940206711)
XLA Ops:
  32.0 13.1 %all_to_all.145 = bf16[4,176,512]{2,1,0:T(8,128)(2,1)S(1)} all-to-all(bf16[4,176,512]{2,1,0:T(8,128)(2,1)S(1)} %broadcast_in_dim.42), channel_id=1, replica_groups=mesh['fs_0'=4,'fs_1'=4,'tp'=4,'rep'=2] {'tp'}, dimensions={0} | all-to-all | bytes 1441792 | tf_op jit(solution)/shard_map/all_to_all | solution.py:31
  69.5 9.5 %all-to-all-done.21 = bf16[32,32,256]{2,1,0:T(8,128)(2,1)S(1)} async-done(((bf16[32,32,256]{2,1,0:T(8,128)(2,1)}), bf16[32,32,256]{2,1,0:T(8,128)(2,1)S(1)}, u32[]{:S(2)}, u32[]{:S(2)}) %all-to-all-start.21) | async-done | bytes 524320 | tf_op jit(solution)/shard_map/all_to_all | solution.py:47
  88.0 25.9 %all-to-all-done.11 = bf16[32,64,512]{2,1,0:T(8,128)(2,1)S(1)} async-done(((bf16[32,64,512]{2,1,0:T(8,128)(2,1)}), bf16[32,64,512]{2,1,0:T(8,128)(2,1)S(1)}, u32[]{:S(2)}, u32[]{:S(2)}) %all-to-all-start.11) | async-done | bytes 2097184 | tf_op jit(solution)/shard_map/all_to_all | solution.py:47
  122.7 26.0 %all-to-all-done.2 = bf16[32,64,512]{2,1,0:T(8,128)(2,1)} async-done(((bf16[32,64,512]{2,1,0:T(8,128)(2,1)}), bf16[32,64,512]{2,1,0:T(8,128)(2,1)}, u32[]{:S(2)}, u32[]{:S(2)}) %all-to-all-start.2) | async-done | bytes 2097184 | tf_op jit(solution)/shard_map/all_to_all | solution.py:47
  159.8 9.6 %all-reduce.1 = (f32[]{:T(128)}, f32[]{:T(128)}, f32[]{:T(128)}, f32[]{:T(128)}, f32[]{:T(128)}, /*index=5*/f32[]{:T(128)}) all-reduce(f32[]{:T(128)} %get-tuple-element.18, f32[]{:T(128)} %get-tuple-element.19, f32[]{:T(128)} %get-tuple-element.20, f32[]{:T(128)} %get-tuple-element.21, ...), channel_id=1, replica_groups=mesh['fs_0'=4,'fs_1'=4,'tp'=4,'rep'=2] {'fs_1'}, use_global_device_ids=true, to_apply=%region_4.0 | all-reduce | flops 6 | bytes 48 | tf_op jit(solution)/shard_map/psum | solution.py:53
  169.4 9.6 %all-reduce = (f32[]{:T(128)}, f32[]{:T(128)}, f32[]{:T(128)}, f32[]{:T(128)}, f32[]{:T(128)}, /*index=5*/f32[]{:T(128)}) all-reduce(f32[]{:T(128)} %get-tuple-element.12, f32[]{:T(128)} %get-tuple-element.13, f32[]{:T(128)} %get-tuple-element.14, f32[]{:T(128)} %get-tuple-element.15, ...), channel_id=1, replica_groups=mesh['fs_0'=4,'fs_1'=4,'tp'=4,'rep'=2] {'tp'}, use_global_device_ids=true, to_apply=%region_5.0 | all-reduce | flops 6 | bytes 48 | tf_op jit(solution)/shard_map/psum | solution.py:53
  186.1 37.8 %all-gather.13.cloned.1.call-done = bf16[2048,512]{1,0:T(8,128)(2,1)} async-done(((bf16[64,512]{1,0:T(8,128)(2,1)}), bf16[2048,512]{1,0:T(8,128)(2,1)}) %all-gather.13.cloned.1.call-update) | async-done | bytes 2097168 | tf_op jit(solution)/shard_map/all_gather | solution.py:81
  231.2 12.0 %all-to-all-done.12 = bf16[4,176,512]{2,1,0:T(8,128)(2,1)S(1)} async-done(((bf16[4,176,512]{2,1,0:T(8,128)(2,1)}), bf16[4,176,512]{2,1,0:T(8,128)(2,1)S(1)}, u32[]{:S(2)}, u32[]{:S(2)}) %all-to-all-start.12) | async-done | bytes 720928 | tf_op jit(solution)/shard_map/all_to_all | solution.py:31
  245.5 13.5 %all_to_all.146 = bf16[4,176,512]{2,1,0:T(8,128)(2,1)S(1)} all-to-all(bf16[4,176,512]{2,1,0:T(8,128)(2,1)S(1)} %broadcast_in_dim.44), channel_id=1, replica_groups=mesh['fs_0'=4,'fs_1'=4,'tp'=4,'rep'=2] {'tp'}, dimensions={0} | all-to-all | bytes 1441792 | tf_op jit(solution)/shard_map/all_to_all | solution.py:31
  259.8 33.5 %all_to_all.147 = bf16[32,64,512]{2,1,0:T(8,128)(2,1)S(1)} all-to-all(bf16[32,64,512]{2,1,0:T(8,128)(2,1)S(1)} %bitcast.134), channel_id=1, replica_groups=mesh['fs_0'=4,'fs_1'=4,'tp'=4,'rep'=2] {'fs_0','fs_1','rep'}, dimensions={0} | all-to-all | bytes 4194304 | tf_op jit(solution)/shard_map/all_to_all | solution.py:47
  301.6 12.0 %all-to-all-done.3 = bf16[4,176,512]{2,1,0:T(8,128)(2,1)S(1)} async-done(((bf16[4,176,512]{2,1,0:T(8,128)(2,1)}), bf16[4,176,512]{2,1,0:T(8,128)(2,1)S(1)}, u32[]{:S(2)}, u32[]{:S(2)}) %all-to-all-start.3) | async-done | bytes 720928 | tf_op jit(solution)/shard_map/all_to_all | solution.py:31
  315.4 13.7 %all_to_all.148 = bf16[4,176,512]{2,1,0:T(8,128)(2,1)S(1)} all-to-all(bf16[4,176,512]{2,1,0:T(8,128)(2,1)S(1)} %broadcast_in_dim.38), channel_id=1, replica_groups=mesh['fs_0'=4,'fs_1'=4,'tp'=4,'rep'=2] {'tp'}, dimensions={0} | all-to-all | bytes 1441792 | tf_op jit(solution)/shard_map/all_to_all | solution.py:31
  330.0 32.8 %all_to_all.149 = bf16[32,64,512]{2,1,0:T(8,128)(2,1)S(1)} all-to-all(bf16[32,64,512]{2,1,0:T(8,128)(2,1)S(1)} %bitcast.135), channel_id=1, replica_groups=mesh['fs_0'=4,'fs_1'=4,'tp'=4,'rep'=2] {'fs_0','fs_1','rep'}, dimensions={0} | all-to-all | bytes 4194304 | tf_op jit(solution)/shard_map/all_to_all | solution.py:47
  366.3 14.7 %all_to_all.150 = bf16[4,176,512]{2,1,0:T(8,128)(2,1)S(1)} all-to-all(bf16[4,176,512]{2,1,0:T(8,128)(2,1)S(1)} %broadcast_in_dim.45), channel_id=1, replica_groups=mesh['fs_0'=4,'fs_1'=4,'tp'=4,'rep'=2] {'tp'}, dimensions={0} | all-to-all | bytes 1441792 | tf_op jit(solution)/shard_map/all_to_all | solution.py:31
  381.6 13.4 %all_to_all.151 = bf16[4,176,512]{2,1,0:T(8,128)(2,1)S(1)} all-to-all(bf16[4,176,512]{2,1,0:T(8,128)(2,1)S(1)} %broadcast_in_dim.46), channel_id=1, replica_groups=mesh['fs_0'=4,'fs_1'=4,'tp'=4,'rep'=2] {'tp'}, dimensions={0} | all-to-all | bytes 1441792 | tf_op jit(solution)/shard_map/all_to_all | solution.py:31
  395.9 33.2 %all_to_all.152 = bf16[32,64,512]{2,1,0:T(8,128)(2,1)S(1)} all-to-all(bf16[32,64,512]{2,1,0:T(8,128)(2,1)S(1)} %bitcast.136), channel_id=1, replica_groups=mesh['fs_0'=4,'fs_1'=4,'tp'=4,'rep'=2] {'fs_0','fs_1','rep'}, dimensions={0} | all-to-all | bytes 4194304 | tf_op jit(solution)/shard_map/all_to_all | solution.py:47
  432.5 14.7 %all_to_all.153 = bf16[4,176,512]{2,1,0:T(8,128)(2,1)S(1)} all-to-all(bf16[4,176,512]{2,1,0:T(8,128)(2,1)S(1)} %broadcast_in_dim.39), channel_id=1, replica_groups=mesh['fs_0'=4,'fs_1'=4,'tp'=4,'rep'=2] {'tp'}, dimensions={0} | all-to-all | bytes 1441792 | tf_op jit(solution)/shard_map/all_to_all | solution.py:31
  447.9 13.4 %all_to_all.154 = bf16[4,176,512]{2,1,0:T(8,128)(2,1)S(1)} all-to-all(bf16[4,176,512]{2,1,0:T(8,128)(2,1)S(1)} %broadcast_in_dim.40), channel_id=1, replica_groups=mesh['fs_0'=4,'fs_1'=4,'tp'=4,'rep'=2] {'tp'}, dimensions={0} | all-to-all | bytes 1441792 | tf_op jit(solution)/shard_map/all_to_all | solution.py:31
  469.8 28.7 %all-to-all-done.8 = bf16[32,64,512]{2,1,0:T(8,128)(2,1)S(1)} async-done(((bf16[32,64,512]{2,1,0:T(8,128)(2,1)}), bf16[32,64,512]{2,1,0:T(8,128)(2,1)S(1)}, u32[]{:S(2)}, u32[]{:S(2)}) %all-to-all-start.8) | async-done | bytes 2097184 | tf_op jit(solution)/shard_map/all_to_all | solution.py:47
  500.2 21.8 %all_gather.33 = bf16[1024,256]{1,0:T(8,128)(2,1)S(1)} all-gather(bf16[32,256]{1,0:T(8,128)(2,1)S(1)} %divide_convert_fusion.2), channel_id=1, replica_groups=mesh['fs_0'=4,'fs_1'=4,'tp'=4,'rep'=2] {'fs_0','fs_1','rep'}, dimensions={0}, use_global_device_ids=true | all-gather | bytes 540672 | tf_op jit(solution)/shard_map/all_gather | solution.py:81
  542.8 17.2 %all_to_all.156 = bf16[32,32,256]{2,1,0:T(8,128)(2,1)S(1)} all-to-all(bf16[32,32,256]{2,1,0:T(8,128)(2,1)S(1)} %bitcast.164), channel_id=1, replica_groups=mesh['fs_0'=4,'fs_1'=4,'tp'=4,'rep'=2] {'fs_0','fs_1','rep'}, dimensions={0} | all-to-all | bytes 1048576 | tf_op jit(solution)/shard_map/all_to_all | solution.py:47
  560.1 22.5 %all_gather.34 = bf16[1024,256]{1,0:T(8,128)(2,1)S(1)} all-gather(bf16[32,256]{1,0:T(8,128)(2,1)S(1)} %reduce_sum.186), channel_id=1, replica_groups=mesh['fs_0'=4,'fs_1'=4,'tp'=4,'rep'=2] {'fs_0','fs_1','rep'}, dimensions={0}, use_global_device_ids=true | all-gather | bytes 540672 | tf_op jit(solution)/shard_map/all_gather | solution.py:81
  600.3 16.4 %all_to_all.159 = bf16[32,32,256]{2,1,0:T(8,128)(2,1)S(1)} all-to-all(bf16[32,32,256]{2,1,0:T(8,128)(2,1)S(1)} %bitcast.165), channel_id=1, replica_groups=mesh['fs_0'=4,'fs_1'=4,'tp'=4,'rep'=2] {'fs_0','fs_1','rep'}, dimensions={0} | all-to-all | bytes 1048576 | tf_op jit(solution)/shard_map/all_to_all | solution.py:47
  616.8 22.8 %all_gather.35 = bf16[1024,256]{1,0:T(8,128)(2,1)S(1)} all-gather(bf16[32,256]{1,0:T(8,128)(2,1)S(1)} %reduce_sum.187), channel_id=1, replica_groups=mesh['fs_0'=4,'fs_1'=4,'tp'=4,'rep'=2] {'fs_0','fs_1','rep'}, dimensions={0}, use_global_device_ids=true | all-gather | bytes 540672 | tf_op jit(solution)/shard_map/all_gather | solution.py:81
  (211 shorter events, 205.8 us)
Async XLA Ops:
  8.7 6.6 all-to-all-start.19
  15.3 5.5 all-to-all-start
  20.3 29.3 %copy-start.31 = (bf16[64,256]{1,0:T(8,128)(2,1)}, bf16[64,256]{1,0:T(8,128)(2,1)S(1)}, u32[]{:S(2)}) copy-start(bf16[64,256]{1,0:T(8,128)(2,1)S(1)} %get-tuple-element.31) | copy-start | bytes 98308
  21.5 10.4 %all-to-all-start.20 = ((bf16[4,64,256]{2,1,0:T(8,128)(2,1)}), bf16[4,64,256]{2,1,0:T(8,128)(2,1)S(1)}, u32[]{:S(2)}, u32[]{:S(2)}) async-start(bf16[4,64,256]{2,1,0:T(8,128)(2,1)} %broadcast_in_dim.48), calls=%async_computation.20 | async-start | bytes 262144 | tf_op jit(solution)/shard_map/all_to_all | solution.py:31
  27.7 39.8 %copy-start.13 = (bf16[176,512]{1,0:T(8,128)(2,1)}, bf16[176,512]{1,0:T(8,128)(2,1)S(1)}, u32[]{:S(2)}) copy-start(bf16[176,512]{1,0:T(8,128)(2,1)S(1)} %get-tuple-element.34) | copy-start | bytes 540676
  46.0 13.0 %all-to-all-start.1 = ((bf16[4,176,512]{2,1,0:T(8,128)(2,1)}), bf16[4,176,512]{2,1,0:T(8,128)(2,1)S(1)}, u32[]{:S(2)}, u32[]{:S(2)}) async-start(bf16[4,176,512]{2,1,0:T(8,128)(2,1)} %broadcast_in_dim.36), calls=%async_computation.1 | async-start | bytes 1441792 | tf_op jit(solution)/shard_map/all_to_all | solution.py:31
  59.1 19.9 %all-to-all-start.21 = ((bf16[32,32,256]{2,1,0:T(8,128)(2,1)}), bf16[32,32,256]{2,1,0:T(8,128)(2,1)S(1)}, u32[]{:S(2)}, u32[]{:S(2)}) async-start(bf16[32,32,256]{2,1,0:T(8,128)(2,1)} %bitcast.24), calls=%async_computation.21 | async-start | bytes 1048576 | tf_op jit(solution)/shard_map/all_to_all | solution.py:47
  79.8 34.1 %all-to-all-start.11 = ((bf16[32,64,512]{2,1,0:T(8,128)(2,1)}), bf16[32,64,512]{2,1,0:T(8,128)(2,1)S(1)}, u32[]{:S(2)}, u32[]{:S(2)}) async-start(bf16[32,64,512]{2,1,0:T(8,128)(2,1)} %bitcast.133), calls=%async_computation.11 | async-start | bytes 4194304 | tf_op jit(solution)/shard_map/all_to_all | solution.py:47
  113.9 34.8 %all-to-all-start.2 = ((bf16[32,64,512]{2,1,0:T(8,128)(2,1)}), bf16[32,64,512]{2,1,0:T(8,128)(2,1)}, u32[]{:S(2)}, u32[]{:S(2)}) async-start(bf16[32,64,512]{2,1,0:T(8,128)(2,1)} %bitcast.132), calls=%async_computation.2 | async-start | bytes 4194304 | tf_op jit(solution)/shard_map/all_to_all | solution.py:47
  118.7 105.2 %all-gather.13.cloned.1.call-start = ((), (), s32[]{:S(2)}) async-start(), calls=%async_computation.32 | async-start | bytes 2162688 | tf_op jit(solution)/shard_map/all_gather | solution.py:81
  122.7 60.7 %copy-start.23 = (f32[64,512]{1,0:T(8,128)S(1)}, f32[64,512]{1,0:T(8,128)}, u32[]{:S(2)}) copy-start(f32[64,512]{1,0:T(8,128)} %copy-done.22) | copy-start | bytes 393220
  184.1 110.2 %all-gather.7.cloned.1.call-start = ((), (), s32[]{:S(2)}) async-start(), calls=%async_computation.29 | async-start | bytes 2162688 | tf_op jit(solution)/shard_map/all_gather | solution.py:81
  226.9 16.2 %all-to-all-start.12 = ((bf16[4,176,512]{2,1,0:T(8,128)(2,1)}), bf16[4,176,512]{2,1,0:T(8,128)(2,1)S(1)}, u32[]{:S(2)}, u32[]{:S(2)}) async-start(bf16[4,176,512]{2,1,0:T(8,128)(2,1)} %broadcast_in_dim.43), calls=%async_computation.12 | async-start | bytes 1441792 | tf_op jit(solution)/shard_map/all_to_all | solution.py:31
  231.2 132.8 %all-gather.15.cloned.1.call-start = ((), (), s32[]{:S(2)}) async-start(), calls=%async_computation.33 | async-start | bytes 2162688 | tf_op jit(solution)/shard_map/all_gather | solution.py:81
  298.1 15.6 %all-to-all-start.3 = ((bf16[4,176,512]{2,1,0:T(8,128)(2,1)}), bf16[4,176,512]{2,1,0:T(8,128)(2,1)S(1)}, u32[]{:S(2)}, u32[]{:S(2)}) async-start(bf16[4,176,512]{2,1,0:T(8,128)(2,1)} %broadcast_in_dim.37), calls=%async_computation.3 | async-start | bytes 1441792 | tf_op jit(solution)/shard_map/all_to_all | solution.py:31
  301.6 128.5 %all-gather.9.cloned.1.call-start = ((), (), s32[]{:S(2)}) async-start(), calls=%async_computation.30 | async-start | bytes 2162688 | tf_op jit(solution)/shard_map/all_gather | solution.py:81
  363.8 280.9 %all-gather.17.cloned.1.call-start = ((), (), s32[]{:S(2)}) async-start(), calls=%async_computation.34 | async-start | bytes 2162688 | tf_op jit(solution)/shard_map/all_gather | solution.py:81
  463.4 35.1 %all-to-all-start.8 = ((bf16[32,64,512]{2,1,0:T(8,128)(2,1)}), bf16[32,64,512]{2,1,0:T(8,128)(2,1)S(1)}, u32[]{:S(2)}, u32[]{:S(2)}) async-start(bf16[32,64,512]{2,1,0:T(8,128)(2,1)} %bitcast.131), calls=%async_computation.8 | async-start | bytes 4194304 | tf_op jit(solution)/shard_map/all_to_all | solution.py:47
  468.4 186.7 %all-gather.11.cloned.1.call-start = ((), (), s32[]{:S(2)}) async-start(), calls=%async_computation.31 | async-start | bytes 2162688 | tf_op jit(solution)/shard_map/all_gather | solution.py:81
  523.8 9.4 %all-to-all-start.22 = ((bf16[4,64,256]{2,1,0:T(8,128)(2,1)}), bf16[4,64,256]{2,1,0:T(8,128)(2,1)S(1)}, u32[]{:S(2)}, u32[]{:S(2)}) async-start(bf16[4,64,256]{2,1,0:T(8,128)(2,1)} %broadcast_in_dim.49), calls=%async_computation.22 | async-start | bytes 262144 | tf_op jit(solution)/shard_map/all_to_all | solution.py:31
  591.6 49.0 %copy-start.32 = (bf16[64,256]{1,0:T(8,128)(2,1)}, bf16[64,256]{1,0:T(8,128)(2,1)S(1)}, u32[]{:S(2)}) copy-start(bf16[64,256]{1,0:T(8,128)(2,1)S(1)} %fusion.43) | copy-start | bytes 98308
  641.3 9.4 %all-to-all-start.28 = ((bf16[4,64,256]{2,1,0:T(8,128)(2,1)}), bf16[4,64,256]{2,1,0:T(8,128)(2,1)S(1)}, u32[]{:S(2)}, u32[]{:S(2)}) async-start(bf16[4,64,256]{2,1,0:T(8,128)(2,1)} %broadcast_in_dim.53), calls=%async_computation.28 | async-start | bytes 262144 | tf_op jit(solution)/shard_map/all_to_all | solution.py:31
  651.6 14.7 %all-to-all-start.18 = ((bf16[4,176,512]{2,1,0:T(8,128)(2,1)}), bf16[4,176,512]{2,1,0:T(8,128)(2,1)S(1)}, u32[]{:S(2)}, u32[]{:S(2)}) async-start(bf16[4,176,512]{2,1,0:T(8,128)(2,1)} %broadcast_in_dim.47), calls=%async_computation.18 | async-start | bytes 1441792 | tf_op jit(solution)/shard_map/all_to_all | solution.py:31
  667.4 13.9 %all-to-all-start.9 = ((bf16[4,176,512]{2,1,0:T(8,128)(2,1)}), bf16[4,176,512]{2,1,0:T(8,128)(2,1)S(1)}, u32[]{:S(2)}, u32[]{:S(2)}) async-start(bf16[4,176,512]{2,1,0:T(8,128)(2,1)} %broadcast_in_dim.41), calls=%async_computation.9 | async-start | bytes 1441792 | tf_op jit(solution)/shard_map/all_to_all | solution.py:31
  (36 other events, 313.7 us)
Sparse Core Ops, SparseCore 0:
  184.2 39.6 all-gather.12
  226.7 42.9 all-gather.6
  294.4 39.9 all-gather.14
  363.9 39.6 all-gather.8
  430.2 39.6 all-gather.16
  499.5 39.2 all-gather.10
where the time goes:
time: 695 us; the launch traced here: 692 us
  blocking collectives  353 us (51%)
  waiting for transfers between devices  189 us (27%)
  starting transfers between devices  58.7 us (8%)
  matrix products  37.4 us (5%)
  between operations  19 us (3%)
  other arithmetic  18.2 us (3%)
  local copies, waits for them, and re-layouts  17.1 us (2%)
    all_to_all x5, blocking collectives, sum_at_owner(): lax.all_to_all(split_up(value, dim, devices), axis, 0, 0, tiled=True)  133 us
    all_to_all x10, blocking collectives, from_everyone(): lax.all_to_all(jnp.broadcast_to(value[None], (devices, *value.shape)), ax...  122 us
    all_to_all x6, waiting for transfers between devices, sum_at_owner(): lax.all_to_all(split_up(value, dim, devices), axis, 0, 0, tiled=True)  90.6 us
    all_gather x3, blocking collectives, spread(): return lax.all_gather(share, FS_REP, axis=0, tiled=True)  67.1 us
    all_to_all x8, waiting for transfers between devices, from_everyone(): lax.all_to_all(jnp.broadcast_to(value[None], (devices, *value.shape)), ax...  60.8 us
    all_gather x6, waiting for transfers between devices, spread(): return lax.all_gather(share, FS_REP, axis=0, tiled=True)  37.9 us
    psum x4, blocking collectives, by_axis(): value = lax.psum(value, axis)  30.8 us
    all_to_all x8, starting transfers between devices, from_everyone(): lax.all_to_all(jnp.broadcast_to(value[None], (devices, *value.shape)), ax...  29.3 us
  transfers between devices with their start and end apart: 20, of which 14 were waited for; matrix products, arithmetic and copies ran while one was open for 8% of the time, Pallas kernels for 0%

commit v1 on v0

--- a/solution.py
+++ b/solution.py
@@ -78,7 +78,10 @@
 
 
 def spread(share):
-    return lax.all_gather(share, FS_REP, axis=0, tiled=True)
+    try_all_quarters = lambda u, row_dim: jnp.concatenate(
+        lax.all_to_all(jnp.stack(lax.axis_size(FS_REP) * [u], 0), FS_REP, 0, 0), row_dim
+    )
+    return try_all_quarters(share, 0)
 
 
 def second_product(ymat, columns):

time: 695 us -> 837 us (1.20)
  waiting for transfers between devices: 189 us -> 475 us
  blocking collectives: 353 us -> 82.4 us
  starting transfers between devices: 58.7 us -> 144 us
  local copies, waits for them, and re-layouts: 17.1 us -> 53.5 us
  between operations: 19 us -> 5.61 us
  matrix products: 37.4 us -> 46.4 us
    all_to_all x0 -> x8, waiting for transfers between devices: none -> 186 us  [spread(): lax.all_to_all(jnp.stack(lax.axis_size(FS_REP) * [u], 0), FS_REP, 0, 0)]
    all_to_all x5 -> x1, blocking collectives: 133 us -> 15.1 us  [sum_at_owner(): lax.all_to_all(split_up(value, dim, devices), axis, 0, 0, tiled=True)]
    all_to_all x10 -> x2, blocking collectives: 122 us -> 21.5 us  [from_everyone(): lax.all_to_all(jnp.broadcast_to(value[None], (devices, *value.shape)), ax...]
    all_to_all x6 -> x10, waiting for transfers between devices: 90.6 us -> 179 us  [sum_at_owner(): lax.all_to_all(split_up(value, dim, devices), axis, 0, 0, tiled=True)]
    all_gather x3 -> x0, blocking collectives: 67.1 us -> none  [spread(): return lax.all_gather(share, FS_REP, axis=0, tiled=True)]
    all_to_all x8 -> x16, waiting for transfers between devices: 60.8 us -> 110 us  [from_everyone(): lax.all_to_all(jnp.broadcast_to(value[None], (devices, *value.shape)), ax...]
    all_gather x6 -> x0, waiting for transfers between devices: 37.9 us -> none  [spread(): return lax.all_gather(share, FS_REP, axis=0, tiled=True)]
    all_to_all x0 -> x8, starting transfers between devices: none -> 33.8 us  [spread(): lax.all_to_all(jnp.stack(lax.axis_size(FS_REP) * [u], 0), FS_REP, 0, 0)]
  transfers between devices with their start and end apart: 20 -> 34, of which waited for: 14 -> 33; matrix products, arithmetic and copies ran while one was open for 8% -> 9% of each run, Pallas kernels for 0% -> 0%
where the time goes in v1:
time: 837 us; the launch traced here: 831 us
  waiting for transfers between devices  475 us (57%)
  starting transfers between devices  144 us (17%)
  blocking collectives  82.4 us (10%)
  local copies, waits for them, and re-layouts  53.5 us (6%)
  matrix products  46.4 us (6%)
  other arithmetic  25.2 us (3%)
    all_to_all x8, waiting for transfers between devices, spread(): lax.all_to_all(jnp.stack(lax.axis_size(FS_REP) * [u], 0), FS_REP, 0, 0)  186 us
    all_to_all x10, waiting for transfers between devices, sum_at_owner(): lax.all_to_all(split_up(value, dim, devices), axis, 0, 0, tiled=True)  179 us
    all_to_all x16, waiting for transfers between devices, from_everyone(): lax.all_to_all(jnp.broadcast_to(value[None], (devices, *value.shape)), ax...  110 us
    all_to_all x16, starting transfers between devices, from_everyone(): lax.all_to_all(jnp.broadcast_to(value[None], (devices, *value.shape)), ax...  56.9 us
    all_to_all x10, starting transfers between devices, sum_at_owner(): lax.all_to_all(split_up(value, dim, devices), axis, 0, 0, tiled=True)  53 us
    all_to_all x8, starting transfers between devices, spread(): lax.all_to_all(jnp.stack(lax.axis_size(FS_REP) * [u], 0), FS_REP, 0, 0)  33.8 us
    psum x4, blocking collectives, by_axis(): value = lax.psum(value, axis)  30.8 us
    all_to_all x2, blocking collectives, from_everyone(): lax.all_to_all(jnp.broadcast_to(value[None], (devices, *value.shape)), ax...  21.5 us
  transfers between devices with their start and end apart: 34, of which 33 were waited for; matrix products, arithmetic and copies ran while one was open for 9% of the time, Pallas kernels for 0%

profile of v1, /device:TPU:0, one launch (start us, length us, event | category | flops | bytes accessed | tf_op | source)
XLA Modules:
  0.0 831.5 jit_solution(3619428140870326873)
XLA Ops:
  25.5 13.1 %all_to_all.190 = bf16[4,176,512]{2,1,0:T(8,128)(2,1)S(1)} all-to-all(bf16[4,176,512]{2,1,0:T(8,128)(2,1)S(1)} %broadcast_in_dim.42), channel_id=1, replica_groups=mesh['fs_0'=4,'fs_1'=4,'tp'=4,'rep'=2] {'tp'}, dimensions={0} | all-to-all | bytes 1441792 | tf_op jit(solution)/shard_map/all_to_all | solution.py:31
  63.2 9.4 %all-to-all-done.27 = bf16[32,32,256]{2,1,0:T(8,128)(2,1)S(1)} async-done(((bf16[32,32,256]{2,1,0:T(8,128)(2,1)}), bf16[32,32,256]{2,1,0:T(8,128)(2,1)S(1)}, u32[]{:S(2)}, u32[]{:S(2)}) %all-to-all-start.27) | async-done | bytes 524320 | tf_op jit(solution)/shard_map/all_to_all | solution.py:47
  81.6 25.9 %all-to-all-done.14 = bf16[32,64,512]{2,1,0:T(8,128)(2,1)S(1)} async-done(((bf16[32,64,512]{2,1,0:T(8,128)(2,1)}), bf16[32,64,512]{2,1,0:T(8,128)(2,1)S(1)}, u32[]{:S(2)}, u32[]{:S(2)}) %all-to-all-start.14) | async-done | bytes 2097184 | tf_op jit(solution)/shard_map/all_to_all | solution.py:47
  116.2 26.1 %all-to-all-done.2 = bf16[32,64,512]{2,1,0:T(8,128)(2,1)} async-done(((bf16[32,64,512]{2,1,0:T(8,128)(2,1)}), bf16[32,64,512]{2,1,0:T(8,128)(2,1)}, u32[]{:S(2)}, u32[]{:S(2)}) %all-to-all-start.2) | async-done | bytes 2097184 | tf_op jit(solution)/shard_map/all_to_all | solution.py:47
  153.9 9.6 %all-reduce.1 = (f32[]{:T(128)}, f32[]{:T(128)}, f32[]{:T(128)}, f32[]{:T(128)}, f32[]{:T(128)}, /*index=5*/f32[]{:T(128)}) all-reduce(f32[]{:T(128)} %get-tuple-element.18, f32[]{:T(128)} %get-tuple-element.19, f32[]{:T(128)} %get-tuple-element.20, f32[]{:T(128)} %get-tuple-element.21, ...), channel_id=1, replica_groups=mesh['fs_0'=4,'fs_1'=4,'tp'=4,'rep'=2] {'fs_1'}, use_global_device_ids=true, to_apply=%region_4.0 | all-reduce | flops 6 | bytes 48 | tf_op jit(solution)/shard_map/psum | solution.py:53
  163.5 9.6 %all-reduce = (f32[]{:T(128)}, f32[]{:T(128)}, f32[]{:T(128)}, f32[]{:T(128)}, f32[]{:T(128)}, /*index=5*/f32[]{:T(128)}) all-reduce(f32[]{:T(128)} %get-tuple-element.12, f32[]{:T(128)} %get-tuple-element.13, f32[]{:T(128)} %get-tuple-element.14, f32[]{:T(128)} %get-tuple-element.15, ...), channel_id=1, replica_groups=mesh['fs_0'=4,'fs_1'=4,'tp'=4,'rep'=2] {'tp'}, use_global_device_ids=true, to_apply=%region_5.0 | all-reduce | flops 6 | bytes 48 | tf_op jit(solution)/shard_map/psum | solution.py:53
  182.5 11.6 %all-to-all-done.28 = bf16[32,32,256]{2,1,0:T(8,128)(2,1)S(1)} async-done(((bf16[32,32,256]{2,1,0:T(8,128)(2,1)}), bf16[32,32,256]{2,1,0:T(8,128)(2,1)S(1)}, u32[]{:S(2)}, u32[]{:S(2)}) %all-to-all-start.28) | async-done | bytes 524320 | tf_op jit(solution)/shard_map/all_to_all | solution.py:82
  213.2 15.1 %all_to_all.192 = bf16[32,32,256]{2,1,0:T(8,128)(2,1)S(1)} all-to-all(bf16[32,32,256]{2,1,0:T(8,128)(2,1)S(1)} %bitcast.187), channel_id=1, replica_groups=mesh['fs_0'=4,'fs_1'=4,'tp'=4,'rep'=2] {'fs_0','fs_1','rep'}, dimensions={0} | all-to-all | bytes 1048576 | tf_op jit(solution)/shard_map/all_to_all | solution.py:47
  228.4 15.1 %all_to_all.193 = bf16[32,32,256]{2,1,0:T(8,128)(2,1)S(1)} all-to-all(bf16[32,32,256]{2,1,0:T(8,128)(2,1)S(1)} %stack.25), channel_id=1, replica_groups=mesh['fs_0'=4,'fs_1'=4,'tp'=4,'rep'=2] {'fs_0','fs_1','rep'}, dimensions={0} | all-to-all | bytes 1048576 | tf_op jit(solution)/shard_map/all_to_all | solution.py:82
  272.3 27.3 %all-to-all-done.15 = bf16[32,64,512]{2,1,0:T(8,128)(2,1)S(1)} async-done(((bf16[32,64,512]{2,1,0:T(8,128)(2,1)}), bf16[32,64,512]{2,1,0:T(8,128)(2,1)S(1)}, u32[]{:S(2)}, u32[]{:S(2)}) %all-to-all-start.15) | async-done | bytes 2097184 | tf_op jit(solution)/shard_map/all_to_all | solution.py:82
  310.2 26.6 %all-to-all-done.3 = bf16[32,64,512]{2,1,0:T(8,128)(2,1)} async-done(((bf16[32,64,512]{2,1,0:T(8,128)(2,1)}), bf16[32,64,512]{2,1,0:T(8,128)(2,1)}, u32[]{:S(2)}, u32[]{:S(2)}) %all-to-all-start.3) | async-done | bytes 2097184 | tf_op jit(solution)/shard_map/all_to_all | solution.py:82
  342.7 10.3 %all-to-all-done.35 = bf16[32,32,256]{2,1,0:T(8,128)(2,1)} async-done(((bf16[32,32,256]{2,1,0:T(8,128)(2,1)}), bf16[32,32,256]{2,1,0:T(8,128)(2,1)}, u32[]{:S(2)}, u32[]{:S(2)}) %all-to-all-start.35) | async-done | bytes 524320 | tf_op jit(solution)/shard_map/all_to_all | solution.py:47
  359.4 11.0 %all-to-all-done.16 = bf16[4,176,512]{2,1,0:T(8,128)(2,1)S(1)} async-done(((bf16[4,176,512]{2,1,0:T(8,128)(2,1)}), bf16[4,176,512]{2,1,0:T(8,128)(2,1)S(1)}, u32[]{:S(2)}, u32[]{:S(2)}) %all-to-all-start.16) | async-done | bytes 720928 | tf_op jit(solution)/shard_map/all_to_all | solution.py:31
  377.7 9.2 %all-to-all-done.36 = bf16[32,32,256]{2,1,0:T(8,128)(2,1)S(1)} async-done(((bf16[32,32,256]{2,1,0:T(8,128)(2,1)}), bf16[32,32,256]{2,1,0:T(8,128)(2,1)S(1)}, u32[]{:S(2)}, u32[]{:S(2)}) %all-to-all-start.36) | async-done | bytes 524320 | tf_op jit(solution)/shard_map/all_to_all | solution.py:82
  452.1 25.8 %all-to-all-done.18 = bf16[32,64,512]{2,1,0:T(8,128)(2,1)S(1)} async-done(((bf16[32,64,512]{2,1,0:T(8,128)(2,1)}), bf16[32,64,512]{2,1,0:T(8,128)(2,1)S(1)}, u32[]{:S(2)}, u32[]{:S(2)}) %all-to-all-start.18) | async-done | bytes 2097184 | tf_op jit(solution)/shard_map/all_to_all | solution.py:47
  485.9 27.6 %all-to-all-done.6 = bf16[32,64,512]{2,1,0:T(8,128)(2,1)S(1)} async-done(((bf16[32,64,512]{2,1,0:T(8,128)(2,1)}), bf16[32,64,512]{2,1,0:T(8,128)(2,1)S(1)}, u32[]{:S(2)}, u32[]{:S(2)}) %all-to-all-start.6) | async-done | bytes 2097184 | tf_op jit(solution)/shard_map/all_to_all | solution.py:47
  522.5 27.6 %all-to-all-done.19 = bf16[32,64,512]{2,1,0:T(8,128)(2,1)S(1)} async-done(((bf16[32,64,512]{2,1,0:T(8,128)(2,1)}), bf16[32,64,512]{2,1,0:T(8,128)(2,1)S(1)}, u32[]{:S(2)}, u32[]{:S(2)}) %all-to-all-start.19) | async-done | bytes 2097184 | tf_op jit(solution)/shard_map/all_to_all | solution.py:82
  559.4 27.3 %all-to-all-done.7 = bf16[32,64,512]{2,1,0:T(8,128)(2,1)S(1)} async-done(((bf16[32,64,512]{2,1,0:T(8,128)(2,1)}), bf16[32,64,512]{2,1,0:T(8,128)(2,1)S(1)}, u32[]{:S(2)}, u32[]{:S(2)}) %all-to-all-start.7) | async-done | bytes 2097184 | tf_op jit(solution)/shard_map/all_to_all | solution.py:82
  593.2 9.1 %all-to-all-done.20 = bf16[4,176,512]{2,1,0:T(8,128)(2,1)S(1)} async-done(((bf16[4,176,512]{2,1,0:T(8,128)(2,1)}), bf16[4,176,512]{2,1,0:T(8,128)(2,1)S(1)}, u32[]{:S(2)}, u32[]{:S(2)}) %all-to-all-start.20) | async-done | bytes 720928 | tf_op jit(solution)/shard_map/all_to_all | solution.py:31
  645.0 11.0 %all-to-all-start.22 = ((bf16[32,64,512]{2,1,0:T(8,128)(2,1)}), bf16[32,64,512]{2,1,0:T(8,128)(2,1)S(1)}, u32[]{:S(2)}, u32[]{:S(2)}) async-start(bf16[32,64,512]{2,1,0:T(8,128)(2,1)} %bitcast.151), calls=%async_computation.22 | async-start | bytes 4194304 | tf_op jit(solution)/shard_map/all_to_all | solution.py:47
  660.2 25.8 %all-to-all-done.22 = bf16[32,64,512]{2,1,0:T(8,128)(2,1)S(1)} async-done(((bf16[32,64,512]{2,1,0:T(8,128)(2,1)}), bf16[32,64,512]{2,1,0:T(8,128)(2,1)S(1)}, u32[]{:S(2)}, u32[]{:S(2)}) %all-to-all-start.22) | async-done | bytes 2097184 | tf_op jit(solution)/shard_map/all_to_all | solution.py:47
  694.0 27.6 %all-to-all-done.10 = bf16[32,64,512]{2,1,0:T(8,128)(2,1)S(1)} async-done(((bf16[32,64,512]{2,1,0:T(8,128)(2,1)}), bf16[32,64,512]{2,1,0:T(8,128)(2,1)S(1)}, u32[]{:S(2)}, u32[]{:S(2)}) %all-to-all-start.10) | async-done | bytes 2097184 | tf_op jit(solution)/shard_map/all_to_all | solution.py:47
  730.8 27.6 %all-to-all-done.23 = bf16[32,64,512]{2,1,0:T(8,128)(2,1)S(1)} async-done(((bf16[32,64,512]{2,1,0:T(8,128)(2,1)}), bf16[32,64,512]{2,1,0:T(8,128)(2,1)S(1)}, u32[]{:S(2)}, u32[]{:S(2)}) %all-to-all-start.23) | async-done | bytes 2097184 | tf_op jit(solution)/shard_map/all_to_all | solution.py:82
  766.8 28.9 %all-to-all-done.11 = bf16[32,64,512]{2,1,0:T(8,128)(2,1)} async-done(((bf16[32,64,512]{2,1,0:T(8,128)(2,1)}), bf16[32,64,512]{2,1,0:T(8,128)(2,1)}, u32[]{:S(2)}, u32[]{:S(2)}) %all-to-all-start.11) | async-done | bytes 2097184 | tf_op jit(solution)/shard_map/all_to_all | solution.py:82
  (248 shorter events, 368.1 us)
Async XLA Ops:
  39.5 13.0 %all-to-all-start.1 = ((bf16[4,176,512]{2,1,0:T(8,128)(2,1)}), bf16[4,176,512]{2,1,0:T(8,128)(2,1)S(1)}, u32[]{:S(2)}, u32[]{:S(2)}) async-start(bf16[4,176,512]{2,1,0:T(8,128)(2,1)} %broadcast_in_dim.36), calls=%async_computation.1 | async-start | bytes 1441792 | tf_op jit(solution)/shard_map/all_to_all | solution.py:31
  52.6 19.9 %all-to-all-start.27 = ((bf16[32,32,256]{2,1,0:T(8,128)(2,1)}), bf16[32,32,256]{2,1,0:T(8,128)(2,1)S(1)}, u32[]{:S(2)}, u32[]{:S(2)}) async-start(bf16[32,32,256]{2,1,0:T(8,128)(2,1)} %bitcast.30), calls=%async_computation.27 | async-start | bytes 1048576 | tf_op jit(solution)/shard_map/all_to_all | solution.py:47
  73.3 34.1 %all-to-all-start.14 = ((bf16[32,64,512]{2,1,0:T(8,128)(2,1)}), bf16[32,64,512]{2,1,0:T(8,128)(2,1)S(1)}, u32[]{:S(2)}, u32[]{:S(2)}) async-start(bf16[32,64,512]{2,1,0:T(8,128)(2,1)} %bitcast.149), calls=%async_computation.14 | async-start | bytes 4194304 | tf_op jit(solution)/shard_map/all_to_all | solution.py:47
  107.5 34.8 %all-to-all-start.2 = ((bf16[32,64,512]{2,1,0:T(8,128)(2,1)}), bf16[32,64,512]{2,1,0:T(8,128)(2,1)}, u32[]{:S(2)}, u32[]{:S(2)}) async-start(bf16[32,64,512]{2,1,0:T(8,128)(2,1)} %bitcast.148), calls=%async_computation.2 | async-start | bytes 4194304 | tf_op jit(solution)/shard_map/all_to_all | solution.py:47
  178.5 15.6 %all-to-all-start.28 = ((bf16[32,32,256]{2,1,0:T(8,128)(2,1)}), bf16[32,32,256]{2,1,0:T(8,128)(2,1)S(1)}, u32[]{:S(2)}, u32[]{:S(2)}) async-start(bf16[32,32,256]{2,1,0:T(8,128)(2,1)} %stack.24), calls=%async_computation.28 | async-start | bytes 1048576 | tf_op jit(solution)/shard_map/all_to_all | solution.py:82
  265.4 34.1 %all-to-all-start.15 = ((bf16[32,64,512]{2,1,0:T(8,128)(2,1)}), bf16[32,64,512]{2,1,0:T(8,128)(2,1)S(1)}, u32[]{:S(2)}, u32[]{:S(2)}) async-start(bf16[32,64,512]{2,1,0:T(8,128)(2,1)} %stack.21), calls=%async_computation.15 | async-start | bytes 4194304 | tf_op jit(solution)/shard_map/all_to_all | solution.py:82
  301.9 34.8 %all-to-all-start.3 = ((bf16[32,64,512]{2,1,0:T(8,128)(2,1)}), bf16[32,64,512]{2,1,0:T(8,128)(2,1)}, u32[]{:S(2)}, u32[]{:S(2)}) async-start(bf16[32,64,512]{2,1,0:T(8,128)(2,1)} %stack.18), calls=%async_computation.3 | async-start | bytes 4194304 | tf_op jit(solution)/shard_map/all_to_all | solution.py:82
  336.8 16.2 %all-to-all-start.35 = ((bf16[32,32,256]{2,1,0:T(8,128)(2,1)}), bf16[32,32,256]{2,1,0:T(8,128)(2,1)}, u32[]{:S(2)}, u32[]{:S(2)}) async-start(bf16[32,32,256]{2,1,0:T(8,128)(2,1)} %bitcast.186), calls=%async_computation.35 | async-start | bytes 1048576 | tf_op jit(solution)/shard_map/all_to_all | solution.py:47
  354.8 15.6 %all-to-all-start.16 = ((bf16[4,176,512]{2,1,0:T(8,128)(2,1)}), bf16[4,176,512]{2,1,0:T(8,128)(2,1)S(1)}, u32[]{:S(2)}, u32[]{:S(2)}) async-start(bf16[4,176,512]{2,1,0:T(8,128)(2,1)} %broadcast_in_dim.43), calls=%async_computation.16 | async-start | bytes 1441792 | tf_op jit(solution)/shard_map/all_to_all | solution.py:31
  371.5 15.5 %all-to-all-start.36 = ((bf16[32,32,256]{2,1,0:T(8,128)(2,1)}), bf16[32,32,256]{2,1,0:T(8,128)(2,1)S(1)}, u32[]{:S(2)}, u32[]{:S(2)}) async-start(bf16[32,32,256]{2,1,0:T(8,128)(2,1)} %stack.26), calls=%async_computation.36 | async-start | bytes 1048576 | tf_op jit(solution)/shard_map/all_to_all | solution.py:82
  388.0 15.7 %all-to-all-start.4 = ((bf16[4,176,512]{2,1,0:T(8,128)(2,1)}), bf16[4,176,512]{2,1,0:T(8,128)(2,1)S(1)}, u32[]{:S(2)}, u32[]{:S(2)}) async-start(bf16[4,176,512]{2,1,0:T(8,128)(2,1)} %broadcast_in_dim.37), calls=%async_computation.4 | async-start | bytes 1441792 | tf_op jit(solution)/shard_map/all_to_all | solution.py:31
  414.6 13.6 %all-to-all-start.17 = ((bf16[4,176,512]{2,1,0:T(8,128)(2,1)}), bf16[4,176,512]{2,1,0:T(8,128)(2,1)S(1)}, u32[]{:S(2)}, u32[]{:S(2)}) async-start(bf16[4,176,512]{2,1,0:T(8,128)(2,1)} %broadcast_in_dim.44), calls=%async_computation.17 | async-start | bytes 1441792 | tf_op jit(solution)/shard_map/all_to_all | solution.py:31
  442.5 35.4 %all-to-all-start.18 = ((bf16[32,64,512]{2,1,0:T(8,128)(2,1)}), bf16[32,64,512]{2,1,0:T(8,128)(2,1)S(1)}, u32[]{:S(2)}, u32[]{:S(2)}) async-start(bf16[32,64,512]{2,1,0:T(8,128)(2,1)} %bitcast.150), calls=%async_computation.18 | async-start | bytes 4194304 | tf_op jit(solution)/shard_map/all_to_all | solution.py:47
  479.3 34.1 %all-to-all-start.6 = ((bf16[32,64,512]{2,1,0:T(8,128)(2,1)}), bf16[32,64,512]{2,1,0:T(8,128)(2,1)S(1)}, u32[]{:S(2)}, u32[]{:S(2)}) async-start(bf16[32,64,512]{2,1,0:T(8,128)(2,1)} %bitcast.152), calls=%async_computation.6 | async-start | bytes 4194304 | tf_op jit(solution)/shard_map/all_to_all | solution.py:47
  515.9 34.1 %all-to-all-start.19 = ((bf16[32,64,512]{2,1,0:T(8,128)(2,1)}), bf16[32,64,512]{2,1,0:T(8,128)(2,1)S(1)}, u32[]{:S(2)}, u32[]{:S(2)}) async-start(bf16[32,64,512]{2,1,0:T(8,128)(2,1)} %stack.22), calls=%async_computation.19 | async-start | bytes 4194304 | tf_op jit(solution)/shard_map/all_to_all | solution.py:82
  552.5 34.1 %all-to-all-start.7 = ((bf16[32,64,512]{2,1,0:T(8,128)(2,1)}), bf16[32,64,512]{2,1,0:T(8,128)(2,1)S(1)}, u32[]{:S(2)}, u32[]{:S(2)}) async-start(bf16[32,64,512]{2,1,0:T(8,128)(2,1)} %stack.19), calls=%async_computation.7 | async-start | bytes 4194304 | tf_op jit(solution)/shard_map/all_to_all | solution.py:82
  588.5 13.9 %all-to-all-start.20 = ((bf16[4,176,512]{2,1,0:T(8,128)(2,1)}), bf16[4,176,512]{2,1,0:T(8,128)(2,1)S(1)}, u32[]{:S(2)}, u32[]{:S(2)}) async-start(bf16[4,176,512]{2,1,0:T(8,128)(2,1)} %broadcast_in_dim.45), calls=%async_computation.20 | async-start | bytes 1441792 | tf_op jit(solution)/shard_map/all_to_all | solution.py:31
  604.4 12.7 %all-to-all-start.8 = ((bf16[4,176,512]{2,1,0:T(8,128)(2,1)}), bf16[4,176,512]{2,1,0:T(8,128)(2,1)S(1)}, u32[]{:S(2)}, u32[]{:S(2)}) async-start(bf16[4,176,512]{2,1,0:T(8,128)(2,1)} %broadcast_in_dim.39), calls=%async_computation.8 | async-start | bytes 1441792 | tf_op jit(solution)/shard_map/all_to_all | solution.py:31
  645.0 41.0 %all-to-all-start.22 = ((bf16[32,64,512]{2,1,0:T(8,128)(2,1)}), bf16[32,64,512]{2,1,0:T(8,128)(2,1)S(1)}, u32[]{:S(2)}, u32[]{:S(2)}) async-start(bf16[32,64,512]{2,1,0:T(8,128)(2,1)} %bitcast.151), calls=%async_computation.22 | async-start | bytes 4194304 | tf_op jit(solution)/shard_map/all_to_all | solution.py:47
  687.4 34.1 %all-to-all-start.10 = ((bf16[32,64,512]{2,1,0:T(8,128)(2,1)}), bf16[32,64,512]{2,1,0:T(8,128)(2,1)S(1)}, u32[]{:S(2)}, u32[]{:S(2)}) async-start(bf16[32,64,512]{2,1,0:T(8,128)(2,1)} %bitcast.153), calls=%async_computation.10 | async-start | bytes 4194304 | tf_op jit(solution)/shard_map/all_to_all | solution.py:47
  724.0 34.3 %all-to-all-start.23 = ((bf16[32,64,512]{2,1,0:T(8,128)(2,1)}), bf16[32,64,512]{2,1,0:T(8,128)(2,1)S(1)}, u32[]{:S(2)}, u32[]{:S(2)}) async-start(bf16[32,64,512]{2,1,0:T(8,128)(2,1)} %stack.23), calls=%async_computation.23 | async-start | bytes 4194304 | tf_op jit(solution)/shard_map/all_to_all | solution.py:82
  760.8 34.8 %all-to-all-start.11 = ((bf16[32,64,512]{2,1,0:T(8,128)(2,1)}), bf16[32,64,512]{2,1,0:T(8,128)(2,1)}, u32[]{:S(2)}, u32[]{:S(2)}) async-start(bf16[32,64,512]{2,1,0:T(8,128)(2,1)} %stack.20), calls=%async_computation.11 | async-start | bytes 4194304 | tf_op jit(solution)/shard_map/all_to_all | solution.py:82
  797.5 14.6 %all-to-all-start.24 = ((bf16[4,176,512]{2,1,0:T(8,128)(2,1)}), bf16[4,176,512]{2,1,0:T(8,128)(2,1)}, u32[]{:S(2)}, u32[]{:S(2)}) async-start(bf16[4,176,512]{2,1,0:T(8,128)(2,1)} %broadcast_in_dim.47), calls=%async_computation.24 | async-start | bytes 1441792 | tf_op jit(solution)/shard_map/all_to_all | solution.py:31
  813.0 12.7 %all-to-all-start.12 = ((bf16[4,176,512]{2,1,0:T(8,128)(2,1)}), bf16[4,176,512]{2,1,0:T(8,128)(2,1)S(1)}, u32[]{:S(2)}, u32[]{:S(2)}) async-start(bf16[4,176,512]{2,1,0:T(8,128)(2,1)} %broadcast_in_dim.41), calls=%async_computation.12 | async-start | bytes 1441792 | tf_op jit(solution)/shard_map/all_to_all | solution.py:31
  (60 other events, 721.1 us)
